TPU v7x, 256 devices: a whole 4x4x8 slice. The times are simulated.
256 devices in a mesh: sp: 16 (over y, x), tp: 16 (over z, core).
Axes of the slice: x: 4, y: 4, z: 8, core: 2. Of those that a mesh axis runs over, the one named last changes fastest.
Arguments:
- layer_in: bfloat16 [5120, 2048], P('sp', 'tp'), may hold values from -6 to 6
- out_cot: bfloat16 [5120, 2048], P('sp', 'tp'), may hold values from -6 to 6
- route_ids: int32 [5120, 2], P('sp'), may hold values from 0 to 15, all different within a row; in each aligned block of 320 rows (0 to 319, 320 to 639, ...) at most 80 rows name the same one
- route_probs: float32 [5120, 2], P('sp'), may hold values from 0.2 to 1
- group_prob: float32 [5120], P('sp'), may hold values from 0.3 to 1
- gate_weight: bfloat16 [16, 2048, 2048], P('sp', 'tp'), may hold values from -0.125 to 0.125
- up_weight: bfloat16 [16, 2048, 2048], P('sp', 'tp'), may hold values from -0.125 to 0.125
- down_weight: bfloat16 [16, 2048, 2048], P('sp', 'tp'), may hold values from -0.125 to 0.125
- out_weight: bfloat16 [2048, 2048], P(None, 'tp'), may hold values from -0.125 to 0.125
- query: bfloat16 [5120, 1024], P('sp', 'tp'), may hold values from -6 to 6
- key_in: bfloat16 [5120, 1024], P('sp', 'tp'), may hold values from -0.75 to 0.75
- value: bfloat16 [5120, 2048], P('sp', 'tp'), may hold values from -6 to 6
- decay_logit: bfloat16 [5120, 1024], P('sp', 'tp'), may hold values from -2.5 to 8.5, as said below
Outputs:
- gate_grad: float32 [16, 2048, 2048], P('sp', 'tp')
- up_grad: float32 [16, 2048, 2048], P('sp', 'tp')
- down_grad: float32 [16, 2048, 2048], P('sp', 'tp')
- proj_grad: float32 [2048, 2048], P('sp', 'tp')
- query_grad: float32 [5120, 1024], P('sp', 'tp')
- key_grad: float32 [5120, 1024], P('sp', 'tp')
- value_grad: float32 [5120, 2048], P('sp', 'tp')
- logit_grad: float32 [5120, 1024], P('sp', 'tp')
Inputs may be any that keep to these rules, and one draw needn't show every extreme that they name: `route_ids`: each row names two different experts of 0 to 15; every expert is named by some row; within each aligned block of 320 rows (the rows of one device) no expert is named more than 80 times, and in some block one expert is named exactly 80 times. `decay_logit`: values lie between -2.5 and 8.5; even heads have pre-activations near 5, odd heads near 1.
All inputs are finite; a program needn't handle non-finite values.
Results may differ from a plain program's by a relative error of at most 0.019.
Values may be sent and summed in bfloat16 or wider, within the bound.
No kernel may reach another device: no remote copies, remote signals or barrier semaphores. Data moves between devices by JAX's collectives and lax.ppermute only.
A program may use at most 128 MiB of HBM per device.

v0:
```python
import jax
import jax.numpy as jnp
from jax import lax
from jax.sharding import PartitionSpec as P

DK = 64
DV = 128
BLOCK = 64
decay_temp = 16.0
highest = lax.Precision.HIGHEST


def side_by_side(arrays, axis, dim, along):
    both = jnp.concatenate(arrays, axis=along)
    filled, at, finished = (lax.all_gather(both, axis, axis=dim, tiled=True), 0, [])
    for a in arrays:
        finished.append(lax.slice_in_dim(filled, at, at + a.shape[along], axis=along))
        at += a.shape[along]
    return tuple(finished)


def side_by_side_2(arrays, axis, split_dim, concat_dim, along):
    widths = [a.shape[along] for a in arrays]
    both = jnp.concatenate(arrays, axis=along)
    filled = lax.all_to_all(both, axis, split_axis=split_dim, concat_axis=concat_dim, tiled=True)
    return tuple(jnp.split(filled, [sum(widths[:k]) for k in range(1, len(widths))], axis=along))


def sent_to_all(x, axis):
    copies = jnp.broadcast_to(x, (lax.axis_size(axis), *x.shape))
    return lax.all_to_all(copies, axis, split_axis=0, concat_axis=0, tiled=True)


def all_in_one(x, axis):
    leaves = jax.tree.leaves(x)
    turns = sorted(range(len(leaves)), key=lambda k: -leaves[k].size)
    width = (1, *leaves[turns[0]].shape)[-1]
    lines = [
        jnp.pad(leaves[k].reshape(-1), (0, -leaves[k].size % width)).reshape(-1, width)
        for k in turns
    ]
    both, at, found = (sent_to_all(jnp.concatenate(lines), axis), 0, {})
    for k, line in zip(turns, lines):
        section = both[:, at : at + len(line)].reshape(len(both), -1)
        found[k] = section[:, : leaves[k].size].reshape(-1, *leaves[k].shape)
        at += len(line)
    numbers = iter(range(len(leaves)))
    return jax.tree.map(lambda _: found[next(numbers)], x)


def folded_in_pairs(pieces, combine):
    while len(jax.tree.leaves(pieces)[0]) > 1:
        pieces = jax.vmap(combine)(
            *(jax.tree.map(lambda part: part[side::2], pieces) for side in (0, 1))
        )
    return jax.tree.map(lambda part: part[0], pieces)


def entering(x, axis, combine, identity, reverse):
    length, index = (lax.axis_size(axis), lax.axis_index(axis))
    passed = jnp.arange(length) > index if reverse else jnp.arange(length) < index

    def kept(part, zero, own):
        part = jnp.where(
            passed.reshape(-1, *(1 for _ in own.shape)),
            part.astype(own.dtype),
            jnp.asarray(zero, own.dtype),
        )
        return part[::-1] if reverse else part

    pieces = all_in_one(
        jax.tree.map(
            lambda part, kind: part.astype(kind),
            x,
            jax.tree.map(lambda a: jnp.bfloat16 if a.dtype == jnp.float32 else a.dtype, x),
        ),
        axis,
    )
    return folded_in_pairs(jax.tree.map(kept, pieces, identity, x), combine)


def in_blocks(x, dim, length):
    lengths = x.shape
    blocks = x.reshape(*lengths[:dim], length, lengths[dim] // length, *lengths[dim + 1 :])
    return jnp.moveaxis(blocks, dim, 0)


def summed_on_arrival(x, axis, dim):
    length = lax.axis_size(axis)
    blocks = lax.all_to_all(in_blocks(x, dim, length), axis, 0, 0, tiled=True)
    return jnp.sum(blocks.astype(jnp.float32), axis=0)


def combine_spans(earlier, later):
    return (earlier[0] * later[0], later[1] + later[0][..., None] * earlier[1])


def contract_rows(left_mat, right_mat):
    return lax.dot_general(
        left_mat, right_mat, (((0,), (0,)), ((), ())), preferred_element_type=jnp.float32
    )


def contract_cols(left_mat, right_mat):
    return lax.dot_general(
        left_mat, right_mat, (((1,), (1,)), ((), ())), preferred_element_type=jnp.float32
    )


def to_blocks(tensor, head_count):
    rows_here = tensor.shape[0]
    return (
        tensor.astype(jnp.float32)
        .reshape(rows_here // BLOCK, BLOCK, head_count, -1)
        .transpose(2, 0, 1, 3)
    )


def from_blocks(tensor):
    head_count, blocks, _, channels = tensor.shape
    return tensor.transpose(1, 2, 0, 3).reshape(blocks * BLOCK, head_count * channels)


def expert_pass(rows_x, rows_cot, gate_mat, up_mat, down_mat):
    full_x, full_cot = side_by_side((rows_x, rows_cot), "tp", 1, 0)
    gate_pre = contract_cols(full_x, gate_mat)
    up_pre = contract_cols(full_x, up_mat)
    sigmoid_gate = jax.nn.sigmoid(gate_pre)
    active = gate_pre * sigmoid_gate
    hidden = (active * up_pre).astype(jnp.bfloat16)
    hidden_cot = contract_cols(full_cot, down_mat)
    up_cot = (hidden_cot * active).astype(jnp.bfloat16)
    gate_cot = (
        hidden_cot * up_pre * sigmoid_gate * (1.0 + gate_pre * (1.0 - sigmoid_gate))
    ).astype(jnp.bfloat16)
    down_g = contract_rows(hidden, full_cot)
    gate_g = contract_rows(gate_cot, full_x)
    up_g = contract_rows(up_cot, full_x)
    dims = (((0,), (1,)), ((), ()))
    first_part = lax.dot_general(gate_mat, gate_cot, dims, preferred_element_type=jnp.float32)
    back_terms = lax.psum_scatter(
        (
            first_part + lax.dot_general(up_mat, up_cot, dims, preferred_element_type=jnp.float32)
        ).astype(jnp.bfloat16),
        "tp",
        scatter_dimension=0,
        tiled=True,
    ).astype(jnp.float32)
    return (gate_g, up_g, down_g, back_terms)


def local(
    layer_in,
    out_cot,
    route_ids,
    route_probs,
    group_prob,
    gate_weight,
    up_weight,
    down_weight,
    out_weight,
    query,
    key_in,
    value,
    decay_logit,
):
    tok_rows = layer_in.shape[0]
    local_cols = layer_in.shape[1]
    experts_all = lax.axis_size("sp")
    capacity = 4 * tok_rows // experts_all
    route_weight = group_prob[:, None] * route_probs / jnp.sum(route_probs, axis=1, keepdims=True)
    chosen = (route_ids[:, :, None] == jnp.arange(experts_all, dtype=jnp.int32)).astype(jnp.int32)
    running = jnp.cumsum(chosen.reshape(2 * tok_rows, experts_all), axis=0).reshape(
        tok_rows, 2, experts_all
    )
    position = jnp.sum((running - 1) * chosen, axis=2)
    slot_ids = route_ids * capacity + position
    matches = (
        slot_ids[None, :, :] == jnp.arange(experts_all * capacity, dtype=jnp.int32)[:, None, None]
    )
    select_x = jnp.any(matches, axis=2).astype(jnp.float32)
    select_cot = jnp.sum(jnp.where(matches, route_weight[None], 0.0), axis=2)
    send_x = jnp.dot(
        select_x.astype(jnp.bfloat16), layer_in, preferred_element_type=jnp.float32
    ).astype(jnp.bfloat16)
    send_cot = jnp.dot(select_cot, out_cot.astype(jnp.float32), precision=highest).astype(
        jnp.bfloat16
    )
    send_x = send_x.reshape(experts_all, capacity, local_cols)
    send_cot = send_cot.reshape(experts_all, capacity, local_cols)
    recv_x, recv_cot = side_by_side_2((send_x, send_cot), "sp", 0, 0, 1)
    head_dev = query.shape[1] // DK
    scaled_query = to_blocks(query, head_dev) * DK ** (-0.5)
    key_blk = to_blocks(key_in, head_dev)
    value_blk = to_blocks(value, head_dev)
    logit_blk = to_blocks(decay_logit, head_dev)
    cumulative = jnp.cumsum(jax.nn.log_sigmoid(logit_blk) / decay_temp, axis=2)
    span_log = cumulative[:, :, -1:, :]
    growth = jnp.exp(cumulative)
    shrink = jnp.exp(-cumulative)
    to_end = jnp.exp(span_log - cumulative)
    query_decayed = scaled_query * growth
    key_back = key_blk * shrink
    key_to_end = key_blk * to_end
    causal = jnp.tril(jnp.ones((BLOCK, BLOCK), dtype=bool))
    scores = jnp.where(
        causal, jnp.einsum("hncd,hnsd->hncs", query_decayed, key_back, precision=highest), 0.0
    )
    within = jnp.einsum("hncs,hnsv->hncv", scores, value_blk, precision=highest)
    block_decay = jnp.moveaxis(jnp.exp(span_log[:, :, 0, :]), 1, 0)
    block_update = jnp.moveaxis(
        jnp.einsum("hncd,hncv->hndv", key_to_end, value_blk, precision=highest), 1, 0
    )
    identity_pair = (
        jnp.ones((head_dev, DK), jnp.float32),
        jnp.zeros((head_dev, DK, DV), jnp.float32),
    )

    def advance(carry_pair, inputs):
        return (combine_spans(carry_pair, inputs), carry_pair)

    span_total, before_pairs = lax.scan(advance, identity_pair, (block_decay, block_update))
    entry_pair = entering(span_total, "sp", combine_spans, identity_pair, False)
    entry_state = entry_pair[1]
    decay_before = jnp.moveaxis(before_pairs[0], 0, 1)
    block_state = decay_before[..., None] * entry_state[:, None] + jnp.moveaxis(
        before_pairs[1], 0, 1
    )
    span_end = span_total[0][..., None] * entry_state + span_total[1]
    outputs = within + jnp.einsum("hncd,hndv->hncv", query_decayed, block_state, precision=highest)
    mixer_out = from_blocks(outputs).astype(jnp.bfloat16)
    gate_mat, up_mat, down_mat = (gate_weight[0], up_weight[0], down_weight[0])
    gate_g, up_g, down_g, back_flat = expert_pass(
        recv_x.reshape(-1, local_cols), recv_cot.reshape(-1, local_cols), gate_mat, up_mat, down_mat
    )
    back_terms = back_flat.reshape(local_cols, experts_all, capacity)
    returned = lax.all_to_all(
        back_terms.astype(jnp.bfloat16), "sp", split_axis=1, concat_axis=1, tiled=True
    ).astype(back_terms.dtype)
    returned = returned.reshape(local_cols, experts_all * capacity)
    routed_sum = lax.dot_general(
        select_x,
        returned,
        (((0,), (1,)), ((), ())),
        precision=highest,
        preferred_element_type=jnp.float32,
    )
    mixed_cot = (out_cot.astype(jnp.float32) + routed_sum).astype(jnp.bfloat16)
    full_cot = lax.all_gather(mixed_cot, "tp", axis=1, tiled=True)
    mixer_cot = jnp.dot(full_cot, out_weight, preferred_element_type=jnp.float32)
    proj_grad = summed_on_arrival(contract_rows(full_cot, mixer_out).astype(jnp.bfloat16), "sp", 0)
    cot_blk = to_blocks(mixer_cot, head_dev)
    block_future = jnp.moveaxis(
        jnp.einsum("hncd,hncv->hndv", query_decayed, cot_blk, precision=highest), 1, 0
    )

    def retreat(carry_pair, inputs):
        return (combine_spans(carry_pair, inputs), carry_pair)

    span_back, after_pairs = lax.scan(
        retreat, identity_pair, (block_decay, block_future), reverse=True
    )
    beyond_pair = entering(span_back, "sp", combine_spans, identity_pair, True)
    future_state = beyond_pair[1]
    decay_after = jnp.moveaxis(after_pairs[0], 0, 1)
    block_future_state = decay_after[..., None] * future_state[:, None] + jnp.moveaxis(
        after_pairs[1], 0, 1
    )
    cot_values = jnp.where(
        causal, jnp.einsum("hncv,hnsv->hncs", cot_blk, value_blk, precision=highest), 0.0
    )
    query_scaled_grad = growth * (
        jnp.einsum("hncv,hndv->hncd", cot_blk, block_state, precision=highest)
        + jnp.einsum("hncs,hnsd->hncd", cot_values, key_back, precision=highest)
    )
    key_part = shrink * jnp.einsum("hncs,hncd->hnsd", cot_values, query_decayed, precision=highest)
    key_grad = key_part + to_end * jnp.einsum(
        "hnsv,hndv->hnsd", value_blk, block_future_state, precision=highest
    )
    value_grad = jnp.einsum("hncs,hncv->hnsv", scores, cot_blk, precision=highest) + jnp.einsum(
        "hnsd,hndv->hnsv", key_to_end, block_future_state, precision=highest
    )
    decay_terms = (scaled_query * query_scaled_grad - key_blk * key_grad).reshape(
        head_dev, tok_rows, DK
    )
    tail_sum = jnp.flip(jnp.cumsum(jnp.flip(decay_terms, 1), axis=1), 1)
    beyond_term = jnp.sum(future_state * span_end, axis=2)
    log_grad = tail_sum + beyond_term[:, None, :]
    logit_flat = logit_blk.reshape(head_dev, tok_rows, DK)
    logit_grad = (
        (log_grad * jax.nn.sigmoid(-logit_flat) / decay_temp)
        .transpose(1, 0, 2)
        .reshape(tok_rows, head_dev * DK)
    )
    query_grad = from_blocks(query_scaled_grad * DK ** (-0.5))
    return (
        gate_g[None],
        up_g[None],
        down_g[None],
        proj_grad,
        query_grad,
        from_blocks(key_grad),
        from_blocks(value_grad),
        logit_grad,
    )


def solution(mesh):
    in_specs = (
        P("sp", "tp"),
        P("sp", "tp"),
        P("sp", None),
        P("sp", None),
        P("sp"),
        P("sp", "tp", None),
        P("sp", "tp", None),
        P("sp", "tp", None),
        P(None, "tp"),
        P("sp", "tp"),
        P("sp", "tp"),
        P("sp", "tp"),
        P("sp", "tp"),
    )
    out_specs = (
        P("sp", "tp", None),
        P("sp", "tp", None),
        P("sp", "tp", None),
        P("sp", "tp"),
        P("sp", "tp"),
        P("sp", "tp"),
        P("sp", "tp"),
        P("sp", "tp"),
    )
    return jax.shard_map(local, mesh=mesh, in_specs=in_specs, out_specs=out_specs, check_vma=False)
```

profile of v0, /device:TPU:32, one launch (start us, length us, event | category | flops | bytes accessed | tf_op | source)
XLA Modules:
  0.0 299.6 jit_solution(3981683871783346753)
XLA Ops:
  8.4 1.4 reduce-window.14
  13.5 2.7 convolution_convert_fusion.1
  16.1 1.4 convolution_convert_fusion.2
  17.5 19.8 %all_to_all.25 = bf16[16,160,128]{2,1,0:T(8,128)(2,1)S(1)} all-to-all(bf16[16,160,128]{2,1,0:T(8,128)(2,1)S(1)} %pad_maximum_fusion), channel_id=1, replica_groups=mesh['sp'=16,'tp'=16] {'sp'}, dimensions={0} | all-to-all | bytes 1310720 | tf_op jit(solution)/shard_map/all_to_all | solution.py:25
  38.5 71.1 %all-gather.3.cloned.1.call-done = bf16[2560,2048]{1,0:T(8,128)(2,1)} async-done(((bf16[2560,128]{1,0:T(8,128)(2,1)}), bf16[2560,2048]{1,0:T(8,128)(2,1)}) %all-gather.3.cloned.1.call-update) | async-done | bytes 10485776 | tf_op jit(solution)/shard_map/all_gather | solution.py:15
  109.6 4.2 %fusion.13 = f32[1280,128]{1,0:T(8,128)S(1)} fusion(bf16[2560,2048]{1,0:T(8,128)(2,1)} %all-gather.3.cloned.1.call-done, bf16[1,128,2048]{2,1,0:T(8,128)(2,1)S(1)} %copy-done), kind=kOutput, calls=%fused_computation.24 | convolution fusion | flops 671088640 | bytes 6422528 | tf_op jit(solution)/shard_map/dot_general | solution.py:105
  113.8 1.3 copy-done.1
  115.2 1.6 fusion.15
  116.8 1.7 multiply_convert_fusion.1
  118.5 1.5 fusion.33
  120.0 3.8 %fusion.4 = bf16[2048,1280]{0,1:T(8,128)(2,1)} fusion(f32[1280,2048]{1,0:T(8,128)S(1)} %fusion.33, bf16[1280,128]{1,0:T(8,128)(2,1)S(1)} %get-tuple-element.412, bf16[1,128,2048]{2,1,0:T(8,128)(2,1)S(1)} %copy-done.6), kind=kOutput, calls=%fused_computation.15 | convolution fusion | flops 676331520 | bytes 16580608 | tf_op jit(solution)/shard_map/dot_general | solution.py:143
  123.8 7.9 %copy.182 = bf16[2048,1280]{1,0:T(8,128)(2,1)} copy(bf16[2048,1280]{0,1:T(8,128)(2,1)} %fusion.4) | data formatting | bytes 10485760
  135.1 6.0 %all-to-all-start.2 = ((bf16[16,65,128]{2,1,0:T(8,128)(2,1)}), bf16[16,65,128]{2,1,0:T(8,128)(2,1)S(1)}, u32[]{:S(2)}, u32[]{:S(2)}) async-start(bf16[16,65,128]{2,1,0:T(8,128)(2,1)} %broadcast_in_dim.136), calls=%async_computation.2 | async-start | bytes 589824 | tf_op jit(solution)/shard_map/all_to_all | solution.py:31
  142.4 8.1 %all-to-all-done.2 = bf16[16,65,128]{2,1,0:T(8,128)(2,1)S(1)} async-done(((bf16[16,65,128]{2,1,0:T(8,128)(2,1)}), bf16[16,65,128]{2,1,0:T(8,128)(2,1)S(1)}, u32[]{:S(2)}, u32[]{:S(2)}) %all-to-all-start.2) | async-done | bytes 266272 | tf_op jit(solution)/shard_map/all_to_all | solution.py:31
  150.6 41.9 %reduce-scatter.4.cloned.1.call-done = bf16[128,1280]{1,0:T(8,128)(2,1)} async-done(((bf16[2048,1280]{1,0:T(8,128)(2,1)}), bf16[128,1280]{1,0:T(8,128)(2,1)}) %reduce-scatter.4.cloned.1.call-update) | async-done | bytes 327696
  192.6 1.9 copy.183
  194.4 6.7 %all-to-all-start.1 = ((bf16[128,16,80]{0,2,1:T(8,128)(2,1)}), bf16[128,16,80]{0,2,1:T(8,128)(2,1)}, u32[]{:S(2)}, u32[]{:S(2)}) async-start(bf16[128,16,80]{0,2,1:T(8,128)(2,1)} %bitcast.12), calls=%async_computation.1 | async-start | bytes 655360 | tf_op jit(solution)/shard_map/all_to_all | solution.py:237
  201.7 8.5 %all-to-all-done.1 = bf16[128,16,80]{0,2,1:T(8,128)(2,1)} async-done(((bf16[128,16,80]{0,2,1:T(8,128)(2,1)}), bf16[128,16,80]{0,2,1:T(8,128)(2,1)}, u32[]{:S(2)}, u32[]{:S(2)}) %all-to-all-start.1) | async-done | bytes 327712 | tf_op jit(solution)/shard_map/all_to_all | solution.py:237
  210.2 2.1 fusion.31
  213.7 4.4 %fusion.18 = f32[1,128,2048]{2,1,0:T(8,128)} fusion(bf16[1280,128]{1,0:T(8,128)(2,1)S(1)} %get-tuple-element.413, bf16[2560,2048]{1,0:T(8,128)(2,1)} %all-gather.3.cloned.1.call-done), kind=kOutput, calls=%fused_computation.31 | convolution fusion | flops 671088640 | bytes 6619136 | tf_op jit(solution)/shard_map/dot_general | solution.py:99
  218.1 4.3 %fusion.21 = f32[1,128,2048]{2,1,0:T(8,128)} fusion(bf16[1280,128]{1,0:T(8,128)(2,1)S(1)} %get-tuple-element.412, bf16[2560,2048]{1,0:T(8,128)(2,1)} %all-gather.3.cloned.1.call-done), kind=kOutput, calls=%fused_computation.32 | convolution fusion | flops 671088640 | bytes 6619136 | tf_op jit(solution)/shard_map/dot_general | solution.py:99
  222.5 4.4 %fusion.24 = f32[1,128,2048]{2,1,0:T(8,128)} fusion(bf16[2560,2048]{1,0:T(8,128)(2,1)} %all-gather.3.cloned.1.call-done, f32[1280,128]{1,0:T(8,128)S(1)} %copy-done.20, f32[1280,128]{1,0:T(8,128)S(1)} %copy-done.18), kind=kOutput, calls=%fused_computation.33 | convolution fusion | flops 672071680 | bytes 7602176 | tf_op jit(solution)/shard_map/dot_general | solution.py:99
  226.9 21.5 %all-gather.5.cloned.1.call-done = bf16[320,2048]{1,0:T(8,128)(2,1)} async-done(((bf16[320,128]{1,0:T(8,128)(2,1)}), bf16[320,2048]{1,0:T(8,128)(2,1)}) %all-gather.5.cloned.1.call-update) | async-done | bytes 1310736 | tf_op jit(solution)/shard_map/all_gather | solution.py:249
  248.4 2.0 fusion.83
  253.5 7.3 %while.42 = (s32[]{:T(128)}, f32[1,64]{1,0:T(1,128)S(1)}, f32[1,64,128]{2,1,0:T(8,128)S(1)}, f32[5,1,64]{2,0,1:T(8,128)S(1)}, f32[5,1,64,128]{3,2,1,0:T(8,128)S(...) while((s32[]{:T(128)}, f32[1,64]{1,0:T(1,128)S(1)}, ...), condition=%wide.region_12.13_spmd.clone, body=%wide.region_11.12_spmd.clone.sunk | while | flops 32900 | bytes 166297 | solution.py:260
  261.5 6.8 %all-to-all-start.4 = ((bf16[16,65,128]{2,1,0:T(8,128)(2,1)}), bf16[16,65,128]{2,1,0:T(8,128)(2,1)S(1)}, u32[]{:S(2)}, u32[]{:S(2)}) async-start(bf16[16,65,128]{2,1,0:T(8,128)(2,1)} %broadcast_in_dim.141), calls=%async_computation.4 | async-start | bytes 589824 | tf_op jit(solution)/shard_map/all_to_all | solution.py:31
  268.3 2.3 convolution_convert_fusion
  271.8 1.9 fusion.29
  273.7 4.1 %all-to-all-done.4 = bf16[16,65,128]{2,1,0:T(8,128)(2,1)S(1)} async-done(((bf16[16,65,128]{2,1,0:T(8,128)(2,1)}), bf16[16,65,128]{2,1,0:T(8,128)(2,1)S(1)}, u32[]{:S(2)}, u32[]{:S(2)}) %all-to-all-start.4) | async-done | bytes 266272 | tf_op jit(solution)/shard_map/all_to_all | solution.py:31
  277.7 3.6 %all-to-all-start.3 = ((bf16[16,128,128]{2,1,0:T(8,128)(2,1)}), bf16[16,128,128]{2,1,0:T(8,128)(2,1)S(1)}, u32[]{:S(2)}, u32[]{:S(2)}) async-start(bf16[16,128,128]{2,1,0:T(8,128)(2,1)} %bitcast.35), calls=%async_computation.3 | async-start | bytes 1048576 | tf_op jit(solution)/shard_map/all_to_all | solution.py:90
  283.4 1.3 multiply_subtract_fusion
  290.9 1.4 all-to-all-done.3
  (214 shorter events, 34.2 us)
Async XLA Ops:
  7.2 102.5 %copy-start = (bf16[1,128,2048]{2,1,0:T(8,128)(2,1)S(1)}, bf16[1,128,2048]{2,1,0:T(8,128)(2,1)}, u32[]{:S(2)}) copy-start(bf16[1,128,2048]{2,1,0:T(8,128)(2,1)} %param.22) | copy-start | bytes 1572868
  7.2 102.4 %all-gather.3.cloned.1.call-start = ((), (), s32[]{:S(2)}) async-start(), calls=%async_computation.6 | async-start | bytes 11141120 | tf_op jit(solution)/shard_map/all_gather | solution.py:15
  11.6 26.6 %copy-start.7 = (pred[1280,320]{0,1:T(8,128)(4,1)}, pred[1280,320]{0,1:T(8,128)(4,1)S(1)}, u32[]{:S(2)}) copy-start(pred[1280,320]{0,1:T(8,128)(4,1)S(1)} %fusion.17) | copy-start | bytes 1228804
  38.3 75.5 %copy-start.6 = (bf16[1,128,2048]{2,1,0:T(8,128)(2,1)S(1)}, bf16[1,128,2048]{2,1,0:T(8,128)(2,1)}, u32[]{:S(2)}) copy-start(bf16[1,128,2048]{2,1,0:T(8,128)(2,1)} %param.23) | copy-start | bytes 1572868
  38.3 154.3 %reduce-scatter.4.cloned.1.call-start = ((), (), s32[]{:S(2)}) async-start(), calls=%async_computation.8 | async-start | bytes 5570560
  109.6 5.5 %copy-start.1 = (bf16[2560,2048]{1,0:T(8,128)(2,1)S(1)}, bf16[2560,2048]{1,0:T(8,128)(2,1)}, u32[]{:S(2)}) copy-start(bf16[2560,2048]{1,0:T(8,128)(2,1)} %all-gather.3.cloned.1.call-done) | copy-start | bytes 31457284
  115.2 1.6 copy-start.17
  115.2 1.6 copy-start.16
  116.7 1.7 copy-start.19
  131.7 0.8 copy-start.8
  131.7 0.9 copy-start.10
  131.7 1.3 copy-start.3
  131.7 9.4 %copy-start.9 = (bf16[320,64]{0,1:T(8,128)(2,1)S(1)}, bf16[320,64]{0,1:T(8,128)(2,1)}, u32[]{:S(2)}) copy-start(bf16[320,64]{0,1:T(8,128)(2,1)} %param.26) | copy-start | bytes 122884
  134.3 6.9 %copy-start.11 = (f32[5,1,64]{2,1,0:T(1,128)}, f32[5,1,64]{2,1,0:T(1,128)S(1)}, u32[]{:S(2)}) copy-start(f32[5,1,64]{2,1,0:T(1,128)S(1)} %get-tuple-element.589) | copy-start | bytes 3844
  134.3 78.2 %copy-start.12 = (f32[1,64]{1,0:T(1,128)}, f32[1,64]{1,0:T(1,128)S(1)}, u32[]{:S(2)}) copy-start(f32[1,64]{1,0:T(1,128)S(1)} %get-tuple-element.194) | copy-start | bytes 772
  135.1 15.4 %all-to-all-start.2 = ((bf16[16,65,128]{2,1,0:T(8,128)(2,1)}), bf16[16,65,128]{2,1,0:T(8,128)(2,1)S(1)}, u32[]{:S(2)}, u32[]{:S(2)}) async-start(bf16[16,65,128]{2,1,0:T(8,128)(2,1)} %broadcast_in_dim.136), calls=%async_computation.2 | async-start | bytes 589824 | tf_op jit(solution)/shard_map/all_to_all | solution.py:31
  194.4 15.8 %all-to-all-start.1 = ((bf16[128,16,80]{0,2,1:T(8,128)(2,1)}), bf16[128,16,80]{0,2,1:T(8,128)(2,1)}, u32[]{:S(2)}, u32[]{:S(2)}) async-start(bf16[128,16,80]{0,2,1:T(8,128)(2,1)} %bitcast.12), calls=%async_computation.1 | async-start | bytes 655360 | tf_op jit(solution)/shard_map/all_to_all | solution.py:237
  201.1 47.3 %all-gather.5.cloned.1.call-start = ((), (), s32[]{:S(2)}) async-start(), calls=%async_computation.7 | async-start | bytes 1392640 | tf_op jit(solution)/shard_map/all_gather | solution.py:249
  212.4 10.1 %copy-start.15 = (f32[64]{0:T(128)}, f32[64]{0:T(128)S(1)}, u32[]{:S(2)}) copy-start(f32[64]{0:T(128)S(1)} %slice_bitcast_fusion.1) | copy-start | bytes 772
  213.7 8.8 %copy-start.18 = (f32[1280,128]{1,0:T(8,128)S(1)}, f32[1280,128]{1,0:T(8,128)}, u32[]{:S(2)}) copy-start(f32[1280,128]{1,0:T(8,128)} %copy-done.17) | copy-start | bytes 1966084
  213.7 8.8 %copy-start.20 = (f32[1280,128]{1,0:T(8,128)S(1)}, f32[1280,128]{1,0:T(8,128)}, u32[]{:S(2)}) copy-start(f32[1280,128]{1,0:T(8,128)} %copy-done.19) | copy-start | bytes 1966084
  222.5 31.0 %copy-start.14 = (f32[1,64]{1,0:T(1,128)S(1)}, f32[1,64]{1,0:T(1,128)}, u32[]{:S(2)}) copy-start(f32[1,64]{1,0:T(1,128)} %custom-call.2) | copy-start | bytes 772
  248.4 19.9 %copy-start.2 = (bf16[320,2048]{1,0:T(8,128)(2,1)S(1)}, bf16[320,2048]{1,0:T(8,128)(2,1)}, u32[]{:S(2)}) copy-start(bf16[320,2048]{1,0:T(8,128)(2,1)} %all-gather.5.cloned.1.call-done) | copy-start | bytes 3932164
  261.5 16.2 %all-to-all-start.4 = ((bf16[16,65,128]{2,1,0:T(8,128)(2,1)}), bf16[16,65,128]{2,1,0:T(8,128)(2,1)S(1)}, u32[]{:S(2)}, u32[]{:S(2)}) async-start(bf16[16,65,128]{2,1,0:T(8,128)(2,1)} %broadcast_in_dim.141), calls=%async_computation.4 | async-start | bytes 589824 | tf_op jit(solution)/shard_map/all_to_all | solution.py:31
  268.3 18.3 %copy-start.13 = (f32[1,64]{1,0:T(1,128)S(1)}, f32[1,64]{1,0:T(1,128)}, u32[]{:S(2)}) copy-start(f32[1,64]{1,0:T(1,128)} %copy-done.12) | copy-start | bytes 772
  271.8 11.7 %copy-start.4 = (f32[5,64,64]{2,1,0:T(8,128)S(1)}, f32[5,64,64]{2,1,0:T(8,128)}, u32[]{:S(2)}) copy-start(f32[5,64,64]{2,1,0:T(8,128)} %convolution_multiply_fusion) | copy-start | bytes 245764
  277.7 14.6 %all-to-all-start.3 = ((bf16[16,128,128]{2,1,0:T(8,128)(2,1)}), bf16[16,128,128]{2,1,0:T(8,128)(2,1)S(1)}, u32[]{:S(2)}, u32[]{:S(2)}) async-start(bf16[16,128,128]{2,1,0:T(8,128)(2,1)} %bitcast.35), calls=%async_computation.3 | async-start | bytes 1048576 | tf_op jit(solution)/shard_map/all_to_all | solution.py:90
  282.9 7.0 %copy-start.5 = (f32[5,64,128]{2,1,0:T(8,128)S(1)}, f32[5,64,128]{2,1,0:T(8,128)}, u32[]{:S(2)}) copy-start(f32[5,64,128]{2,1,0:T(8,128)} %fusion.84) | copy-start | bytes 491524
Sparse Core Ops, SparseCore 0:
  38.4 71.1 all-gather.2
  131.9 60.6 reduce-scatter.3
  212.5 35.8 all-gather.4
where the time goes:
time: 301 us; the launch traced here: 300 us
  waiting for transfers between devices  157 us (52%)
  matrix products  46.6 us (15%)
  starting transfers between devices  23.5 us (8%)
  local copies, waits for them, and re-layouts  22.1 us (7%)
  blocking collectives  19.8 us (7%)
  other arithmetic  16.2 us (5%)
  between operations  14.5 us (5%)
    all_gather x1, waiting for transfers between devices, side_by_side(): lax.all_gather(both, axis, axis=dim, tiled=True)  71.1 us
    unnamed x4, waiting for transfers between devices  42 us
    all_gather x1, waiting for transfers between devices, local(): full_cot = lax.all_gather(mixed_cot, 'tp', axis=1, tiled=True)  21.5 us
    all_to_all x1, blocking collectives, side_by_side_2(): lax.all_to_all(both, axis, split_axis=split_dim, concat_axis=concat_dim,...  19.8 us
    dot_general x4, matrix products, contract_rows(): lax.dot_general(left_mat, right_mat, (((0,), (0,)), ((), ())), preferred_...  15.5 us
    unnamed x52, local copies, waits for them, and re-layouts  14.8 us
    all_to_all x2, starting transfers between devices, sent_to_all(): return lax.all_to_all(copies, axis, split_axis=0, concat_axis=0, tiled=True)  12.8 us
    all_to_all x2, waiting for transfers between devices, sent_to_all(): return lax.all_to_all(copies, axis, split_axis=0, concat_axis=0, tiled=True)  12.1 us
  transfers between devices with their start and end apart: 7, of which 7 were waited for; matrix products, arithmetic and copies ran while one was open for 11% of the time, Pallas kernels for 0%

commit v1 on v0

--- a/solution.py
+++ b/solution.py
@@ -246,7 +246,9 @@
         preferred_element_type=jnp.float32,
     )
     mixed_cot = (out_cot.astype(jnp.float32) + routed_sum).astype(jnp.bfloat16)
-    full_cot = lax.all_gather(mixed_cot, "tp", axis=1, tiled=True)
+    full_cot = jnp.concatenate(
+        lax.all_to_all(jnp.stack([mixed_cot] * lax.axis_size("tp")), "tp", 0, 0), axis=1
+    )
     mixer_cot = jnp.dot(full_cot, out_weight, preferred_element_type=jnp.float32)
     proj_grad = summed_on_arrival(contract_rows(full_cot, mixer_out).astype(jnp.bfloat16), "sp", 0)
     cot_blk = to_blocks(mixer_cot, head_dev)

time: 301 us -> 318 us (1.056)
  local copies, waits for them, and re-layouts: 22.1 us -> 28.4 us
  other arithmetic: 16.2 us -> 21.9 us
  starting transfers between devices: 23.5 us -> 28.1 us
    all_gather x1 -> x0, waiting for transfers between devices: 21.5 us -> none  [local(): full_cot = lax.all_gather(mixed_cot, 'tp', axis=1, tiled=True)]
    all_to_all x0 -> x1, waiting for transfers between devices: none -> 14.1 us  [local(): lax.all_to_all(jnp.stack([mixed_cot] * lax.axis_size('tp')), 'tp', 0, 0)]
    unnamed x4 -> x3, waiting for transfers between devices: 42 us -> 50.4 us
    all_to_all x0 -> x1, starting transfers between devices: none -> 8.02 us  [local(): lax.all_to_all(jnp.stack([mixed_cot] * lax.axis_size('tp')), 'tp', 0, 0)]
    all_to_all x2, waiting for transfers between devices: 12.1 us -> 7.29 us  [sent_to_all(): return lax.all_to_all(copies, axis, split_axis=0, concat_axis=0, tiled=True)]
    another operation x12 -> x14, local copies, waits for them, and re-layouts: 0.59 us -> 4.27 us
    unnamed x52 -> x70, local copies, waits for them, and re-layouts: 14.8 us -> 14.8 us
  transfers between devices with their start and end apart: 7 -> 7, of which waited for: 7 -> 6; matrix products, arithmetic and copies ran while one was open for 11% -> 10% of each run, Pallas kernels for 0% -> 0%
where the time goes in v1:
time: 318 us; the launch traced here: 314 us
  waiting for transfers between devices  155 us (49%)
  matrix products  45.6 us (14%)
  local copies, waits for them, and re-layouts  28.4 us (9%)
  starting transfers between devices  28.1 us (9%)
  other arithmetic  21.9 us (7%)
  blocking collectives  19.8 us (6%)
  between operations  14.8 us (5%)
    all_gather x1, waiting for transfers between devices, side_by_side(): lax.all_gather(both, axis, axis=dim, tiled=True)  71.1 us
    unnamed x3, waiting for transfers between devices  50.4 us
    all_to_all x1, blocking collectives, side_by_side_2(): lax.all_to_all(both, axis, split_axis=split_dim, concat_axis=concat_dim,...  19.8 us
    unnamed x70, local copies, waits for them, and re-layouts  14.8 us
    dot_general x4, matrix products, contract_rows(): lax.dot_general(left_mat, right_mat, (((0,), (0,)), ((), ())), preferred_...  14.7 us
    all_to_all x1, waiting for transfers between devices, local(): lax.all_to_all(jnp.stack([mixed_cot] * lax.axis_size('tp')), 'tp', 0, 0)  14.1 us
    all_to_all x2, starting transfers between devices, sent_to_all(): return lax.all_to_all(copies, axis, split_axis=0, concat_axis=0, tiled=True)  9.62 us
    all_to_all x1, waiting for transfers between devices, local(): lax.all_to_all(back_terms.astype(jnp.bfloat16), 'sp', split_axis=1, conca...  8.12 us
  transfers between devices with their start and end apart: 7, of which 6 were waited for; matrix products, arithmetic and copies ran while one was open for 10% of the time, Pallas kernels for 0%

profile of v1, /device:TPU:32, one launch (start us, length us, event | category | flops | bytes accessed | tf_op | source)
XLA Modules:
  0.0 313.7 jit_solution(16199070898529048399)
XLA Ops:
  8.4 1.4 reduce-window.14
  14.8 2.7 convolution_convert_fusion.1
  17.5 19.8 %all_to_all.30 = bf16[16,160,128]{2,1,0:T(8,128)(2,1)S(1)} all-to-all(bf16[16,160,128]{2,1,0:T(8,128)(2,1)S(1)} %pad_maximum_fusion), channel_id=1, replica_groups=mesh['sp'=16,'tp'=16] {'sp'}, dimensions={0} | all-to-all | bytes 1310720 | tf_op jit(solution)/shard_map/all_to_all | solution.py:25
  38.5 71.1 %all-gather.2.cloned.1.call-done = bf16[2560,2048]{1,0:T(8,128)(2,1)} async-done(((bf16[2560,128]{1,0:T(8,128)(2,1)}), bf16[2560,2048]{1,0:T(8,128)(2,1)}) %all-gather.2.cloned.1.call-update) | async-done | bytes 10485776 | tf_op jit(solution)/shard_map/all_gather | solution.py:15
  109.6 4.2 %fusion.13 = f32[1280,128]{1,0:T(8,128)S(1)} fusion(bf16[2560,2048]{1,0:T(8,128)(2,1)} %all-gather.2.cloned.1.call-done, bf16[1,128,2048]{2,1,0:T(8,128)(2,1)S(1)} %copy-done), kind=kOutput, calls=%fused_computation.24 | convolution fusion | flops 671088640 | bytes 6422528 | tf_op jit(solution)/shard_map/dot_general | solution.py:105
  115.1 1.6 fusion.15
  116.7 1.7 multiply_convert_fusion.1
  118.5 1.5 fusion.37
  120.0 3.8 %fusion.4 = bf16[2048,1280]{0,1:T(8,128)(2,1)} fusion(f32[1280,2048]{1,0:T(8,128)S(1)} %fusion.37, bf16[1280,128]{1,0:T(8,128)(2,1)S(1)} %get-tuple-element.434, bf16[1,128,2048]{2,1,0:T(8,128)(2,1)S(1)} %copy-done.14), kind=kOutput, calls=%fused_computation.15 | convolution fusion | flops 676331520 | bytes 16580608 | tf_op jit(solution)/shard_map/dot_general | solution.py:143
  123.8 7.9 %copy.221 = bf16[2048,1280]{1,0:T(8,128)(2,1)} copy(bf16[2048,1280]{0,1:T(8,128)(2,1)} %fusion.4) | data formatting | bytes 10485760
  135.0 6.0 %all-to-all-start.3 = ((bf16[16,65,128]{2,1,0:T(8,128)(2,1)}), bf16[16,65,128]{2,1,0:T(8,128)(2,1)S(1)}, u32[]{:S(2)}, u32[]{:S(2)}) async-start(bf16[16,65,128]{2,1,0:T(8,128)(2,1)} %broadcast_in_dim.136), calls=%async_computation.3 | async-start | bytes 589824 | tf_op jit(solution)/shard_map/all_to_all | solution.py:31
  142.2 50.3 %reduce-scatter.4.cloned.1.call-done = bf16[128,1280]{1,0:T(8,128)(2,1)} async-done(((bf16[2048,1280]{1,0:T(8,128)(2,1)}), bf16[128,1280]{1,0:T(8,128)(2,1)}) %reduce-scatter.4.cloned.1.call-update) | async-done | bytes 327696
  192.5 1.9 copy.222
  194.4 6.6 %all-to-all-start.1 = ((bf16[128,16,80]{0,2,1:T(8,128)(2,1)}), bf16[128,16,80]{0,2,1:T(8,128)(2,1)S(1)}, u32[]{:S(2)}, u32[]{:S(2)}) async-start(bf16[128,16,80]{0,2,1:T(8,128)(2,1)} %bitcast.12), calls=%async_computation.1 | async-start | bytes 655360 | tf_op jit(solution)/shard_map/all_to_all | solution.py:237
  202.0 8.1 %all-to-all-done.1 = bf16[128,16,80]{0,2,1:T(8,128)(2,1)S(1)} async-done(((bf16[128,16,80]{0,2,1:T(8,128)(2,1)}), bf16[128,16,80]{0,2,1:T(8,128)(2,1)S(1)}, u32[]{:S(2)}, u32[]{:S(2)}) %all-to-all-start.1) | async-done | bytes 327712 | tf_op jit(solution)/shard_map/all_to_all | solution.py:237
  211.8 8.0 %all-to-all-start.2 = ((bf16[16,320,128]{2,1,0:T(8,128)(2,1)}), bf16[16,320,128]{2,1,0:T(8,128)(2,1)S(1)}, u32[]{:S(2)}, u32[]{:S(2)}) async-start(bf16[16,320,128]{2,1,0:T(8,128)(2,1)} %stack.2), calls=%async_computation.2 | async-start | bytes 2621440 | tf_op jit(solution)/shard_map/all_to_all | solution.py:250
  222.7 4.5 %fusion.21 = f32[1,128,2048]{2,1,0:T(8,128)} fusion(bf16[1280,128]{1,0:T(8,128)(2,1)} %copy-done.10, bf16[2560,2048]{1,0:T(8,128)(2,1)} %all-gather.2.cloned.1.call-done), kind=kOutput, calls=%fused_computation.32 | convolution fusion | flops 671088640 | bytes 6619136 | tf_op jit(solution)/shard_map/dot_general | solution.py:99
  227.2 4.3 %fusion.18 = f32[1,128,2048]{2,1,0:T(8,128)} fusion(bf16[1280,128]{1,0:T(8,128)(2,1)S(1)} %get-tuple-element.435, bf16[2560,2048]{1,0:T(8,128)(2,1)} %all-gather.2.cloned.1.call-done), kind=kOutput, calls=%fused_computation.31 | convolution fusion | flops 671088640 | bytes 6619136 | tf_op jit(solution)/shard_map/dot_general | solution.py:99
  231.6 4.4 %fusion.24 = f32[1,128,2048]{2,1,0:T(8,128)} fusion(bf16[2560,2048]{1,0:T(8,128)(2,1)} %all-gather.2.cloned.1.call-done, f32[1280,128]{1,0:T(8,128)S(1)} %copy-done.29, f32[1280,128]{1,0:T(8,128)S(1)} %copy-done.27), kind=kOutput, calls=%fused_computation.33 | convolution fusion | flops 672071680 | bytes 7602176 | tf_op jit(solution)/shard_map/dot_general | solution.py:99
  235.9 14.1 %all-to-all-done.2 = bf16[16,320,128]{2,1,0:T(8,128)(2,1)S(1)} async-done(((bf16[16,320,128]{2,1,0:T(8,128)(2,1)}), bf16[16,320,128]{2,1,0:T(8,128)(2,1)S(1)}, u32[]{:S(2)}, u32[]{:S(2)}) %all-to-all-start.2) | async-done | bytes 1310752 | tf_op jit(solution)/shard_map/all_to_all | solution.py:250
  250.0 1.9 copy.195
  252.0 2.4 reshape.482
  254.3 1.5 fusion.35
  255.9 2.1 fusion.87
  259.4 9.9 %while.42 = (s32[]{:T(128)}, f32[1,64]{1,0:T(1,128)}, f32[1,64,128]{2,1,0:T(8,128)S(1)}, f32[5,1,64]{2,0,1:T(8,128)S(1)}, f32[5,1,64,128]{3,2,1,0:T(8,128)S(1)},...) while((s32[]{:T(128)}, f32[1,64]{1,0:T(1,128)}, ...), condition=%wide.region_12.13_spmd.clone, body=%wide.region_11.12_spmd.clone.sunk | while | flops 32900 | bytes 166297 | solution.py:262
  270.7 3.7 %all-to-all-start.5 = ((bf16[16,65,128]{2,1,0:T(8,128)(2,1)}), bf16[16,65,128]{2,1,0:T(8,128)(2,1)S(1)}, u32[]{:S(2)}, u32[]{:S(2)}) async-start(bf16[16,65,128]{2,1,0:T(8,128)(2,1)} %broadcast_in_dim.141), calls=%async_computation.5 | async-start | bytes 589824 | tf_op jit(solution)/shard_map/all_to_all | solution.py:31
  276.9 7.3 %all-to-all-done.5 = bf16[16,65,128]{2,1,0:T(8,128)(2,1)S(1)} async-done(((bf16[16,65,128]{2,1,0:T(8,128)(2,1)}), bf16[16,65,128]{2,1,0:T(8,128)(2,1)S(1)}, u32[]{:S(2)}, u32[]{:S(2)}) %all-to-all-start.5) | async-done | bytes 266272 | tf_op jit(solution)/shard_map/all_to_all | solution.py:31
  286.7 1.5 fusion.50
  288.1 1.4 fusion.32
  289.9 1.4 convolution_convert_fusion
  291.3 3.6 %all-to-all-start.4 = ((bf16[16,128,128]{2,1,0:T(8,128)(2,1)}), bf16[16,128,128]{2,1,0:T(8,128)(2,1)S(1)}, u32[]{:S(2)}, u32[]{:S(2)}) async-start(bf16[16,128,128]{2,1,0:T(8,128)(2,1)} %bitcast.292), calls=%async_computation.4 | async-start | bytes 1048576 | tf_op jit(solution)/shard_map/all_to_all | solution.py:90
  302.1 4.0 %all-to-all-done.4 = bf16[16,128,128]{2,1,0:T(8,128)(2,1)S(1)} async-done(((bf16[16,128,128]{2,1,0:T(8,128)(2,1)}), bf16[16,128,128]{2,1,0:T(8,128)(2,1)S(1)}, u32[]{:S(2)}, u32[]{:S(2)}) %all-to-all-start.4) | async-done | bytes 524320 | tf_op jit(solution)/shard_map/all_to_all | solution.py:90
  (233 shorter events, 44.9 us)
Async XLA Ops:
  7.2 102.4 %copy-start = (bf16[1,128,2048]{2,1,0:T(8,128)(2,1)S(1)}, bf16[1,128,2048]{2,1,0:T(8,128)(2,1)}, u32[]{:S(2)}) copy-start(bf16[1,128,2048]{2,1,0:T(8,128)(2,1)} %param.22) | copy-start | bytes 1572868
  7.2 102.4 %all-gather.2.cloned.1.call-start = ((), (), s32[]{:S(2)}) async-start(), calls=%async_computation.7 | async-start | bytes 11141120 | tf_op jit(solution)/shard_map/all_gather | solution.py:15
  38.2 75.5 %copy-start.14 = (bf16[1,128,2048]{2,1,0:T(8,128)(2,1)S(1)}, bf16[1,128,2048]{2,1,0:T(8,128)(2,1)}, u32[]{:S(2)}) copy-start(bf16[1,128,2048]{2,1,0:T(8,128)(2,1)} %param.23) | copy-start | bytes 1572868
  38.2 154.3 %reduce-scatter.4.cloned.1.call-start = ((), (), s32[]{:S(2)}) async-start(), calls=%async_computation.8 | async-start | bytes 5570560
  109.6 5.5 %copy-start.1 = (bf16[2560,2048]{1,0:T(8,128)(2,1)S(1)}, bf16[2560,2048]{1,0:T(8,128)(2,1)}, u32[]{:S(2)}) copy-start(bf16[2560,2048]{1,0:T(8,128)(2,1)} %all-gather.2.cloned.1.call-done) | copy-start | bytes 31457284
  115.1 1.6 copy-start.26
  115.1 1.6 copy-start.25
  116.7 1.8 copy-start.28
  131.7 9.3 %copy-start.18 = (bf16[320,64]{0,1:T(8,128)(2,1)S(1)}, bf16[320,64]{0,1:T(8,128)(2,1)}, u32[]{:S(2)}) copy-start(bf16[320,64]{0,1:T(8,128)(2,1)} %param.26) | copy-start | bytes 122884
  131.7 78.4 %copy-start.17 = (bf16[320,128]{1,0:T(8,128)(2,1)S(1)}, bf16[320,128]{1,0:T(8,128)(2,1)}, u32[]{:S(2)}) copy-start(bf16[320,128]{1,0:T(8,128)(2,1)} %param.18) | copy-start | bytes 245764
  134.2 7.0 %copy-start.7 = (f32[5,1,64,128]{3,2,1,0:T(8,128)}, f32[5,1,64,128]{3,2,1,0:T(8,128)S(1)}, u32[]{:S(2)}) copy-start(f32[5,1,64,128]{3,2,1,0:T(8,128)S(1)} %get-tuple-element.195) | copy-start | bytes 491524
  134.2 87.5 %copy-start.22 = (f32[5,1,64]{2,1,0:T(1,128)}, f32[5,1,64]{2,1,0:T(1,128)S(1)}, u32[]{:S(2)}) copy-start(f32[5,1,64]{2,1,0:T(1,128)S(1)} %get-tuple-element.613) | copy-start | bytes 3844
  134.2 87.5 %copy-start.23 = (f32[1,64]{1,0:T(1,128)}, f32[1,64]{1,0:T(1,128)S(1)}, u32[]{:S(2)}) copy-start(f32[1,64]{1,0:T(1,128)S(1)} %get-tuple-element.194) | copy-start | bytes 772
  135.0 59.4 %all-to-all-start.3 = ((bf16[16,65,128]{2,1,0:T(8,128)(2,1)}), bf16[16,65,128]{2,1,0:T(8,128)(2,1)S(1)}, u32[]{:S(2)}, u32[]{:S(2)}) async-start(bf16[16,65,128]{2,1,0:T(8,128)(2,1)} %broadcast_in_dim.136), calls=%async_computation.3 | async-start | bytes 589824 | tf_op jit(solution)/shard_map/all_to_all | solution.py:31
  141.1 70.7 %copy-start.4 = (f32[320,64]{1,0:T(8,128)}, f32[320,64]{1,0:T(8,128)S(1)}, u32[]{:S(2)}) copy-start(f32[320,64]{1,0:T(8,128)S(1)} %copy.196) | copy-start | bytes 245764
  141.2 70.6 %copy-start.2 = (f32[5,64,64]{2,1,0:T(8,128)}, f32[5,64,64]{2,1,0:T(8,128)S(1)}, u32[]{:S(2)}) copy-start(f32[5,64,64]{2,1,0:T(8,128)S(1)} %fusion.47) | copy-start | bytes 245764
  142.2 85.0 %copy-start.6 = (f32[5,64,64]{2,1,0:T(8,128)}, f32[5,64,64]{2,1,0:T(8,128)S(1)}, u32[]{:S(2)}) copy-start(f32[5,64,64]{2,1,0:T(8,128)S(1)} %convolution_select_fusion.1) | copy-start | bytes 245764
  194.4 17.4 %copy-start.11 = (bf16[16,65,128]{2,1,0:T(8,128)(2,1)}, bf16[16,65,128]{2,1,0:T(8,128)(2,1)S(1)}, u32[]{:S(2)}) copy-start(bf16[16,65,128]{2,1,0:T(8,128)(2,1)S(1)} %all-to-all-done.3) | copy-start | bytes 798724
  194.4 15.7 %all-to-all-start.1 = ((bf16[128,16,80]{0,2,1:T(8,128)(2,1)}), bf16[128,16,80]{0,2,1:T(8,128)(2,1)S(1)}, u32[]{:S(2)}, u32[]{:S(2)}) async-start(bf16[128,16,80]{0,2,1:T(8,128)(2,1)} %bitcast.12), calls=%async_computation.1 | async-start | bytes 655360 | tf_op jit(solution)/shard_map/all_to_all | solution.py:237
  211.8 38.2 %all-to-all-start.2 = ((bf16[16,320,128]{2,1,0:T(8,128)(2,1)}), bf16[16,320,128]{2,1,0:T(8,128)(2,1)S(1)}, u32[]{:S(2)}, u32[]{:S(2)}) async-start(bf16[16,320,128]{2,1,0:T(8,128)(2,1)} %stack.2), calls=%async_computation.2 | async-start | bytes 2621440 | tf_op jit(solution)/shard_map/all_to_all | solution.py:250
  222.7 8.9 %copy-start.27 = (f32[1280,128]{1,0:T(8,128)S(1)}, f32[1280,128]{1,0:T(8,128)}, u32[]{:S(2)}) copy-start(f32[1280,128]{1,0:T(8,128)} %copy-done.26) | copy-start | bytes 1966084
  222.7 8.9 %copy-start.29 = (f32[1280,128]{1,0:T(8,128)S(1)}, f32[1280,128]{1,0:T(8,128)}, u32[]{:S(2)}) copy-start(f32[1280,128]{1,0:T(8,128)} %copy-done.28) | copy-start | bytes 1966084
  255.9 2.1 copy-start.3
  270.7 25.5 %copy-start.5 = (f32[320,64]{1,0:T(8,128)S(1)}, f32[320,64]{1,0:T(8,128)}, u32[]{:S(2)}) copy-start(f32[320,64]{1,0:T(8,128)} %copy-done.4) | copy-start | bytes 245764
  270.7 25.5 %copy-start.9 = (bf16[320,128]{1,0:T(8,128)(2,1)S(1)}, bf16[320,128]{1,0:T(8,128)(2,1)}, u32[]{:S(2)}) copy-start(bf16[320,128]{1,0:T(8,128)(2,1)} %param.28) | copy-start | bytes 245764
  270.7 25.5 %copy-start.21 = (f32[5,1,64]{2,0,1:T(8,128)S(1)}, f32[5,1,64]{2,0,1:T(8,128)}, u32[]{:S(2)}) copy-start(f32[5,1,64]{2,0,1:T(8,128)} %copy-done.20) | copy-start | bytes 3844
  270.7 13.6 %all-to-all-start.5 = ((bf16[16,65,128]{2,1,0:T(8,128)(2,1)}), bf16[16,65,128]{2,1,0:T(8,128)(2,1)S(1)}, u32[]{:S(2)}, u32[]{:S(2)}) async-start(bf16[16,65,128]{2,1,0:T(8,128)(2,1)} %broadcast_in_dim.141), calls=%async_computation.5 | async-start | bytes 589824 | tf_op jit(solution)/shard_map/all_to_all | solution.py:31
  289.9 8.5 %copy-start.13 = (f32[2,1,64,128]{3,2,0,1:T(8,128)S(1)}, f32[2,1,64,128]{3,2,0,1:T(8,128)}, u32[]{:S(2)}) copy-start(f32[2,1,64,128]{3,2,0,1:T(8,128)} %multiply_add_fusion.5) | copy-start | bytes 196612
  289.9 8.5 %copy-start.24 = (f32[1,64]{1,0:T(1,128)S(1)}, f32[1,64]{1,0:T(1,128)}, u32[]{:S(2)}) copy-start(f32[1,64]{1,0:T(1,128)} %copy-done.23) | copy-start | bytes 772
  289.9 10.5 %copy-start.16 = (bf16[320,64]{0,1:T(8,128)(2,1)S(1)}, bf16[320,64]{0,1:T(8,128)(2,1)}, u32[]{:S(2)}) copy-start(bf16[320,64]{0,1:T(8,128)(2,1)} %param.29) | copy-start | bytes 122884
  289.9 11.2 %copy-start.12 = (f32[5,64,128]{2,1,0:T(8,128)S(1)}, f32[5,64,128]{2,1,0:T(8,128)}, u32[]{:S(2)}) copy-start(f32[5,64,128]{2,1,0:T(8,128)} %fusion.87) | copy-start | bytes 491524
  291.3 14.8 %all-to-all-start.4 = ((bf16[16,128,128]{2,1,0:T(8,128)(2,1)}), bf16[16,128,128]{2,1,0:T(8,128)(2,1)S(1)}, u32[]{:S(2)}, u32[]{:S(2)}) async-start(bf16[16,128,128]{2,1,0:T(8,128)(2,1)} %bitcast.292), calls=%async_computation.4 | async-start | bytes 1048576 | tf_op jit(solution)/shard_map/all_to_all | solution.py:90
  (5 other events, 5.5 us)
Sparse Core Ops, SparseCore 0:
  38.4 71.1 all-gather.1
  131.8 60.6 reduce-scatter.3
